TPU v7x, 32 devices: a whole 2x2x4 slice. The times are simulated.
32 devices in a mesh: ep: 16 (over z, x, core), tp: 2 (over y).
Axes of the slice: x: 2, y: 2, z: 4, core: 2. Of those that a mesh axis runs over, the one named last changes fastest.
Arguments:
- residual_in: bfloat16 [240, 1536], P('ep'), may hold values from -6 to 6
- rec_state: bfloat16 [240, 12, 128, 128], P('ep', 'tp'), may hold values from -6 to 6
- mix_gain: float32 [1536], replicated, may hold values from 0.1 to 1.9
- w_query: bfloat16 [1536, 1536], P('tp', 'ep'), may hold values from -0.15625 to 0.15625
- w_forget: bfloat16 [1536, 1536], P('tp', 'ep'), may hold values from -0.15625 to 0.15625
- w_input: bfloat16 [1536, 1536], P('tp', 'ep'), may hold values from -0.15625 to 0.15625
- w_gate: bfloat16 [1536, 1536], P('tp', 'ep'), may hold values from -0.15625 to 0.15625
- lower_bound: float32 [1536], P('tp'), may hold values from 0 to 0.9
- head_gain: float32 [128], replicated, may hold values from 0.1 to 1.9
- w_out: bfloat16 [1536, 1536], P('tp', 'ep'), may hold values from -0.15625 to 0.15625
- ffn_gain: float32 [1536], replicated, may hold values from 0.1 to 1.9
- route_ids: int32 [240, 6], P('ep'), may hold values from 0 to 15, all different within a row; in each aligned block of 15 rows (0 to 14, 15 to 29, ...) at most 6 rows name the same one
- route_weight: float32 [240, 6], P('ep'), may hold values from 0.2 to 1
- expert_gate: bfloat16 [16, 1536, 512], P('ep', None, 'tp'), may hold values from -0.15625 to 0.15625
- expert_up: bfloat16 [16, 1536, 512], P('ep', None, 'tp'), may hold values from -0.15625 to 0.15625
- expert_down: bfloat16 [16, 512, 1536], P('ep', 'tp'), may hold values from -0.25 to 0.25
Outputs:
- layer_out: bfloat16 [240, 1536], P('ep', 'tp')
- new_state: bfloat16 [240, 12, 128, 128], P('ep', 'tp')
Inputs may be any that keep to these rules, and one draw needn't show every extreme that they name: `route_ids`: each row names 6 different experts. Among the rows of one device no expert is named more than 6 times, and in every draw some device names some expert exactly 6 times.
All inputs are finite; a program needn't handle non-finite values.
Results may differ from a plain program's by a relative error of at most 0.016.
Values may be sent and summed in bfloat16 or wider, within the bound.
A program may use at most 64 MiB of HBM per device.

v0:
```python
import jax
import jax.numpy as jnp
from jax import lax
from jax.sharding import PartitionSpec as P

rms_eps = 1e-06


def rms_scale(values, gain):
    return values * lax.rsqrt(jnp.mean(values * values, axis=-1, keepdims=True) + rms_eps) * gain


def rounded(values):
    return lax.optimization_barrier(values.astype(jnp.bfloat16)).astype(jnp.float32)


def recurrence(lower_bound, head_gain, state_block, query_raw, forget_raw, input_raw, gate_raw):
    seq_count = state_block.shape[0]
    heads_local = state_block.shape[1]
    head_size = state_block.shape[2]
    head_shape = (seq_count, heads_local, head_size)
    forget = lower_bound + (1.0 - lower_bound) * jax.nn.sigmoid(forget_raw)
    query_act = jax.nn.silu(query_raw).reshape(head_shape)
    key_act = (1.0 - forget).reshape(head_shape)
    forget_heads = forget.reshape(head_shape)
    value_act = input_raw.reshape(head_shape)
    state_next = (
        forget_heads[:, :, :, None] * state_block.astype(jnp.float32)
        + key_act[:, :, :, None] * value_act[:, :, None, :]
    )
    readout = jnp.einsum("shk,shkv->shv", query_act, state_next, precision=lax.Precision.HIGHEST)
    gate_heads = jax.nn.silu(gate_raw).reshape(head_shape)
    heads_out = rms_scale(readout, head_gain) * gate_heads
    return (
        state_next.astype(jnp.bfloat16),
        heads_out.reshape(seq_count, heads_local * head_size).astype(jnp.bfloat16),
    )


def shards(
    residual_in,
    rec_state,
    mix_gain,
    w_query,
    w_forget,
    w_input,
    w_gate,
    lower_bound,
    head_gain,
    w_out,
    ffn_gain,
    route_ids,
    route_weight,
    expert_gate,
    expert_up,
    expert_down,
):
    tp_count = lax.axis_size("tp")
    tp_rank = lax.axis_index("tp")
    ep_count = lax.axis_size("ep")
    seq_count = residual_in.shape[0]
    model_width = residual_in.shape[1]
    quarter = model_width // tp_count
    residual = residual_in.astype(jnp.float32)
    normed = rms_scale(residual, mix_gain).astype(jnp.bfloat16)
    own_rows = lax.dynamic_slice_in_dim(normed, tp_rank * quarter, quarter, 1)
    rows_piece = lax.all_gather(own_rows, "ep", axis=0, tiled=True)
    partial_proj = jnp.stack(
        [
            jnp.dot(rows_piece, weight, preferred_element_type=jnp.float32)
            for weight in (w_query, w_forget, w_input, w_gate)
        ],
        axis=1,
    )
    arrived = lax.all_to_all(partial_proj, "ep", split_axis=0, concat_axis=2, tiled=True)
    summed = lax.psum_scatter(arrived, "tp", scatter_dimension=2, tiled=True)
    projected = rounded(summed)
    new_state, heads_out = recurrence(
        lower_bound,
        head_gain,
        rec_state,
        projected[:, 0],
        projected[:, 1],
        projected[:, 2],
        projected[:, 3],
    )
    partial_mix = jnp.dot(
        lax.all_gather(heads_out, "ep", axis=0, tiled=True),
        w_out,
        preferred_element_type=jnp.float32,
    )
    mixed_home = lax.all_to_all(
        partial_mix.astype(jnp.bfloat16), "ep", split_axis=0, concat_axis=1, tiled=True
    ).astype(partial_mix.dtype)
    mixed = lax.psum(mixed_home.astype(jnp.bfloat16), "tp").astype(jnp.float32)
    after_mix = rounded(residual + mixed)
    normed_ffn = rms_scale(after_mix, ffn_gain).astype(jnp.bfloat16)
    exp_dev = expert_gate.shape[0]
    experts_all = ep_count * exp_dev
    top_count = route_ids.shape[1]
    capacity = max(2, seq_count * top_count // experts_all + 1)
    flat_ids = route_ids.reshape(-1)
    onehot = (flat_ids[:, None] == jnp.arange(experts_all, dtype=jnp.int32)[None, :]).astype(
        jnp.int32
    )
    slot_rank = jnp.sum(jnp.cumsum(onehot, axis=0) * onehot, axis=1) - 1
    slot_index = flat_ids * capacity + slot_rank
    placer_int = (
        jnp.arange(experts_all * capacity, dtype=jnp.int32)[:, None] == slot_index[None, :]
    ).astype(jnp.int32)
    placer = jnp.sum(
        placer_int.reshape(experts_all * capacity, seq_count, top_count), axis=2
    ).astype(jnp.bfloat16)
    buffer = (
        jnp.dot(placer, normed_ffn, preferred_element_type=jnp.float32)
        .astype(jnp.bfloat16)
        .reshape(experts_all, capacity, model_width)
    )
    received = lax.all_to_all(buffer, "ep", split_axis=0, concat_axis=0, tiled=True)
    slot_count = received.shape[1]
    grouped = received.reshape(ep_count, exp_dev, slot_count, model_width)
    gate_part = jnp.einsum(
        "sjnd,jdf->sjnf", grouped, expert_gate, preferred_element_type=jnp.float32
    )
    up_part = jnp.einsum("sjnd,jdf->sjnf", grouped, expert_up, preferred_element_type=jnp.float32)
    hidden = (jax.nn.silu(gate_part) * up_part).astype(jnp.bfloat16)
    down_part = jnp.einsum(
        "sjnf,jfd->sjnd", hidden, expert_down, preferred_element_type=jnp.float32
    )
    summed_down = lax.psum_scatter(
        down_part.astype(jnp.bfloat16), "tp", scatter_dimension=3, tiled=True
    )
    returned = summed_down.reshape(experts_all, slot_count, quarter)
    gathered_back = lax.all_to_all(returned, "ep", split_axis=0, concat_axis=0, tiled=True)
    flat_back = gathered_back.reshape(experts_all * capacity, quarter)
    picked = (
        jnp.take(flat_back, slot_index, axis=0)
        .astype(jnp.float32)
        .reshape(seq_count, top_count, quarter)
    )
    expert_sum = jnp.sum(route_weight[:, :, None] * picked, axis=1)
    own_mix = lax.dynamic_slice_in_dim(after_mix, tp_rank * quarter, quarter, 1)
    layer_out = (own_mix + expert_sum).astype(jnp.bfloat16)
    return (layer_out, new_state)


def solution(mesh):
    in_specs = (
        P("ep", None),
        P("ep", "tp", None, None),
        P(),
        P("tp", "ep"),
        P("tp", "ep"),
        P("tp", "ep"),
        P("tp", "ep"),
        P("tp"),
        P(),
        P("tp", "ep"),
        P(),
        P("ep", None),
        P("ep", None),
        P("ep", None, "tp"),
        P("ep", None, "tp"),
        P("ep", "tp", None),
    )
    out_specs = (P("ep", "tp"), P("ep", "tp", None, None))
    return jax.shard_map(shards, mesh=mesh, in_specs=in_specs, out_specs=out_specs, check_vma=False)
```

profile of v0, /device:TPU:0, one launch (start us, length us, event | category | flops | bytes accessed | tf_op | source)
XLA Modules:
  0.0 206.5 jit_solution(8427857682327721564)
XLA Ops:
  7.2 0.0 copy-start
  7.2 0.9 convert_element_type.76
  8.1 0.9 multiply_reduce_fusion.2
  9.0 0.8 dynamic-slice
  9.8 0.1 fusion.36
  9.9 24.1 %all-gather = bf16[16,15,768]{2,1,0:T(8,128)(2,1)S(1)} all-gather(bf16[1,15,768]{2,1,0:T(8,128)(2,1)S(1)} %fusion.36), channel_id=1, replica_groups=mesh['ep'=16,'tp'=2] {'ep'}, dimensions={0}, use_global_device_ids=true | all-gather | bytes 391680 | tf_op jit(solution)/shard_map/all_gather | solution.py:67
  34.0 0.1 reshape.208
  34.1 1.2 convolution_bitcast_fusion.2
  35.3 1.2 convolution_bitcast_fusion.3
  36.5 1.2 convolution_bitcast_fusion.4
  37.7 1.2 convolution_bitcast_fusion.5
  38.9 1.0 copy.50
  39.9 3.6 %all-to-all-start = ((f32[240,4,96]{2,1,0:T(4,128)}), f32[240,4,96]{2,1,0:T(4,128)S(1)}, u32[]{:S(2)}, u32[]{:S(2)}) async-start(f32[240,4,96]{2,1,0:T(4,128)} %copy.50), calls=%async_computation | async-start | bytes 983040 | tf_op jit(solution)/shard_map/all_to_all | solution.py:75
  43.4 0.0 reduce-scatter.7.cloned.1.call-start
  43.5 0.1 copy.55
  43.6 0.1 reshape.191
  43.7 0.1 fusion.31
  43.8 0.1 reduce_window_sum.11
  43.9 13.2 %all-to-all-done = f32[240,4,96]{2,1,0:T(4,128)S(1)} async-done(((f32[240,4,96]{2,1,0:T(4,128)}), f32[240,4,96]{2,1,0:T(4,128)S(1)}, u32[]{:S(2)}, u32[]{:S(2)}) %all-to-all-start) | async-done | bytes 368672 | tf_op jit(solution)/shard_map/all_to_all | solution.py:75
  57.2 7.4 %copy.65 = f32[15,4,16,96]{1,0,3,2:T(8,128)} copy(f32[15,4,16,96]{3,1,0,2:T(4,128)S(1)} %bitcast.97) | data formatting | bytes 737280
  64.5 9.6 %reshape.217 = f32[1536,60]{1,0:T(8,128)} reshape(f32[1536,15,4]{2,1,0:T(8,128)} %bitcast.95) | data formatting | bytes 737280
  74.2 0.0 reduce-scatter.7.cloned.1.call-update
  74.2 0.2 select_reduce_fusion
  74.4 0.1 sub.25
  74.5 0.1 copy.57
  74.6 16.6 %reduce-scatter.7.cloned.1.call-done = f32[768,60]{1,0:T(8,128)} async-done(((f32[1536,60]{1,0:T(8,128)}), f32[768,60]{1,0:T(8,128)}) %reduce-scatter.7.cloned.1.call-update) | async-done | bytes 184336
  91.1 5.3 %reshape.218 = bf16[768,15,4]{2,1,0:T(8,128)(2,1)} reshape(f32[768,60]{1,0:T(8,128)} %reduce-scatter.7.cloned.1.call-done) | data formatting | bytes 276480
  96.4 4.4 %copy.64 = bf16[15,4,768]{2,1,0:T(4,128)(2,1)S(1)} copy(bf16[15,4,768]{1,0,2:T(8,128)(2,1)} %bitcast.96) | data formatting | bytes 184320
  100.9 0.6 slice_reduce_fusion
  101.4 0.0 copy-start.1
  101.6 8.9 %fusion.1 = f32[15,6,1,128]{3,2,1,0:T(1,128)S(1)} fusion(bf16[15,6,128,128]{3,2,1,0:T(8,128)(2,1)} %param.17, f32[15,6,128]{2,1,0:T(8,128)S(1)} %mul.167, f32[15,6,128]{2,1,0:T(8,128)S(1)} %get-tuple-element.8, f32[15,6,128]{2,1,0:T(8,128)S(1)} %get-tuple-element.9, f32[15,6,128,1]{2,1,0,3:T(8,128)S(1)} %multiply_bitcast_fusion), kind=kOutput, calls=%fused_computation.3 | convolution fusion | flops 23592960 | bytes 3179520 | tf_op jit(solution)/shard_map/shk,shkv->shv/dot_general | solution.py:31
  110.5 0.1 fusion.22
  110.6 0.1 fusion.25
  110.7 0.1 reshape.209
  110.8 22.4 %all-gather.1 = bf16[16,15,768]{2,1,0:T(8,128)(2,1)S(1)} all-gather(bf16[1,15,768]{2,1,0:T(8,128)(2,1)S(1)} %reshape.209), channel_id=1, replica_groups=mesh['ep'=16,'tp'=2] {'ep'}, dimensions={0}, use_global_device_ids=true | all-gather | bytes 391680 | tf_op jit(solution)/shard_map/all_gather | solution.py:88
  133.2 0.1 reshape.210
  133.3 1.2 convolution_convert_fusion.2
  134.5 0.1 copy.52
  134.6 0.7 all_to_all.37
  135.3 3.5 %all-to-all-start.1 = ((bf16[16,15,96]{2,1,0:T(8,128)(2,1)}), bf16[16,15,96]{2,1,0:T(8,128)(2,1)S(1)}, u32[]{:S(2)}, u32[]{:S(2)}) async-start(bf16[16,15,96]{2,1,0:T(8,128)(2,1)} %all_to_all.37), calls=%async_computation.1 | async-start | bytes 131072 | tf_op jit(solution)/shard_map/all_to_all | solution.py:92
  138.8 0.0 reduce-scatter.5.cloned.1.call-start
  138.8 0.1 convert_reduce_fusion
  138.9 6.7 %all-to-all-done.1 = bf16[16,15,96]{2,1,0:T(8,128)(2,1)S(1)} async-done(((bf16[16,15,96]{2,1,0:T(8,128)(2,1)}), bf16[16,15,96]{2,1,0:T(8,128)(2,1)S(1)}, u32[]{:S(2)}, u32[]{:S(2)}) %all-to-all-start.1) | async-done | bytes 46112 | tf_op jit(solution)/shard_map/all_to_all | solution.py:92
  145.7 0.1 all_to_all.40
  145.8 7.7 %psum.7 = bf16[15,1536]{1,0:T(8,128)(2,1)S(1)} all-reduce(bf16[15,1536]{1,0:T(8,128)(2,1)S(1)} %all_to_all.40), channel_id=1, replica_groups=mesh['ep'=16,'tp'=2] {'tp'}, use_global_device_ids=true, to_apply=%region_3.4 | all-reduce | flops 23040 | bytes 92160 | tf_op jit(solution)/shard_map/psum | solution.py:95
  153.5 0.1 multiply_reduce_fusion.1
  153.6 0.3 convolution_convert_fusion
  153.9 0.1 reshape.192
  154.0 14.8 %all_to_all.47 = bf16[16,6,1536]{2,1,0:T(8,128)(2,1)S(1)} all-to-all(bf16[16,6,1536]{2,1,0:T(8,128)(2,1)S(1)} %reshape.192), channel_id=1, replica_groups=mesh['ep'=16,'tp'=2] {'ep'}, dimensions={0} | all-to-all | bytes 589824 | tf_op jit(solution)/shard_map/all_to_all | solution.py:119
  168.8 0.3 convolution_bitcast_fusion.1
  169.1 1.4 fusion.5
  170.5 0.0 reduce-scatter.5.cloned.1.call-update
  170.5 0.1 mul.188
  170.6 0.1 copy.54
  170.7 11.0 %reduce-scatter.5.cloned.1.call-done = bf16[16,1,6,768]{3,0,2,1:T(8,128)(2,1)} async-done(((bf16[16,1,6,1536]{3,0,2,1:T(8,128)(2,1)}), bf16[16,1,6,768]{3,0,2,1:T(8,128)(2,1)}) %reduce-scatter.5.cloned.1.call-update) | async-done | bytes 147472 | tf_op jit(solution)/shard_map/reduce_scatter | solution.py:130
  181.7 1.6 copy.60
  183.3 5.6 %all-to-all-start.3 = ((bf16[16,6,768]{2,1,0:T(8,128)(2,1)}), bf16[16,6,768]{2,1,0:T(8,128)(2,1)S(1)}, u32[]{:S(2)}, u32[]{:S(2)}) async-start(bf16[16,6,768]{2,1,0:T(8,128)(2,1)} %copy.60), calls=%async_computation.4 | async-start | bytes 393216 | tf_op jit(solution)/shard_map/all_to_all | solution.py:134
  188.9 6.7 %fusion = bf16[15,6,128,128]{3,2,1,0:T(8,128)(2,1)} fusion(bf16[15,6,128,128]{3,2,1,0:T(8,128)(2,1)} %param.17, f32[15,6,128]{2,1,0:T(8,128)S(1)} %mul.167, f32[15,6,128]{2,1,0:T(8,128)S(1)} %get-tuple-element.8, f32[15,6,128]{2,1,0:T(8,128)S(1)} %get-tuple-element.9), kind=kLoop, calls=%fused_computation.2 | loop fusion | flops 7372800 | bytes 6036480 | tf_op jit(solution)/shard_map/convert_element_type | solution.py:35
  195.6 2.3 %all-to-all-done.3 = bf16[16,6,768]{2,1,0:T(8,128)(2,1)S(1)} async-done(((bf16[16,6,768]{2,1,0:T(8,128)(2,1)}), bf16[16,6,768]{2,1,0:T(8,128)(2,1)S(1)}, u32[]{:S(2)}, u32[]{:S(2)}) %all-to-all-start.3) | async-done | bytes 147488 | tf_op jit(solution)/shard_map/all_to_all | solution.py:134
  197.9 0.1 reshape.198
  197.9 0.8 gather_fusion
  198.7 0.1 gather.7
  198.8 0.2 multiply_reduce_fusion
  199.0 0.6 add_convert_fusion.1
  (36 shorter events, 0.3 us)
Async XLA Ops:
  7.2 161.9 %copy-start = (bf16[1,256,1536]{2,1,0:T(8,128)(2,1)S(1)}, bf16[1,256,1536]{2,1,0:T(8,128)(2,1)}, u32[]{:S(2)}) copy-start(bf16[1,256,1536]{2,1,0:T(8,128)(2,1)} %param.31) | copy-start | bytes 2359300
  7.2 36.3 %copy-start.6 = (s32[15,6]{0,1:T(8,128)S(1)}, s32[15,6]{0,1:T(8,128)}, u32[]{:S(2)}) copy-start(s32[15,6]{0,1:T(8,128)} %param.27) | copy-start | bytes 1084
  39.9 17.3 %all-to-all-start = ((f32[240,4,96]{2,1,0:T(4,128)}), f32[240,4,96]{2,1,0:T(4,128)S(1)}, u32[]{:S(2)}, u32[]{:S(2)}) async-start(f32[240,4,96]{2,1,0:T(4,128)} %copy.50), calls=%async_computation | async-start | bytes 983040 | tf_op jit(solution)/shard_map/all_to_all | solution.py:75
  43.4 47.7 %reduce-scatter.7.cloned.1.call-start = ((), (), s32[]{:S(2)}) async-start(), calls=%async_computation.7 | async-start | bytes 1179648
  64.5 10.0 %copy-start.4 = (f32[768]{0:T(1024)S(1)}, f32[768]{0:T(1024)}, u32[]{:S(2)}) copy-start(f32[768]{0:T(1024)} %param.23) | copy-start | bytes 9220
  96.4 14.2 %copy-start.8 = (f32[128]{0:T(128)S(1)}, f32[128]{0:T(128)}, u32[]{:S(2)}) copy-start(f32[128]{0:T(128)} %param.24) | copy-start | bytes 1540
  100.8 52.7 %copy-start.3 = (bf16[15,1536]{1,0:T(8,128)(2,1)S(1)}, bf16[15,1536]{1,0:T(8,128)(2,1)}, u32[]{:S(2)}) copy-start(bf16[15,1536]{1,0:T(8,128)(2,1)} %param.16) | copy-start | bytes 138244
  100.8 52.8 %copy-start.5 = (f32[1536]{0:T(1024)S(1)}, f32[1536]{0:T(1024)}, u32[]{:S(2)}) copy-start(f32[1536]{0:T(1024)} %param.26) | copy-start | bytes 18436
  101.4 67.4 %copy-start.1 = (bf16[1,1536,256]{2,1,0:T(8,128)(2,1)S(1)}, bf16[1,1536,256]{2,1,0:T(8,128)(2,1)}, u32[]{:S(2)}) copy-start(bf16[1,1536,256]{2,1,0:T(8,128)(2,1)} %param.29) | copy-start | bytes 2359300
  101.5 67.6 %copy-start.2 = (bf16[1,1536,256]{2,1,0:T(8,128)(2,1)S(1)}, bf16[1,1536,256]{2,1,0:T(8,128)(2,1)}, u32[]{:S(2)}) copy-start(bf16[1,1536,256]{2,1,0:T(8,128)(2,1)} %param.30) | copy-start | bytes 2359300
  101.5 69.0 %copy-start.7 = (f32[15,6]{0,1:T(8,128)S(1)}, f32[15,6]{0,1:T(8,128)}, u32[]{:S(2)}) copy-start(f32[15,6]{0,1:T(8,128)} %param.28) | copy-start | bytes 1084
  135.3 10.4 %all-to-all-start.1 = ((bf16[16,15,96]{2,1,0:T(8,128)(2,1)}), bf16[16,15,96]{2,1,0:T(8,128)(2,1)S(1)}, u32[]{:S(2)}, u32[]{:S(2)}) async-start(bf16[16,15,96]{2,1,0:T(8,128)(2,1)} %all_to_all.37), calls=%async_computation.1 | async-start | bytes 131072 | tf_op jit(solution)/shard_map/all_to_all | solution.py:92
  138.8 42.9 %reduce-scatter.5.cloned.1.call-start = ((), (), s32[]{:S(2)}) async-start(), calls=%async_computation.6 | async-start | bytes 442368 | tf_op jit(solution)/shard_map/reduce_scatter | solution.py:130
  183.3 14.6 %all-to-all-start.3 = ((bf16[16,6,768]{2,1,0:T(8,128)(2,1)}), bf16[16,6,768]{2,1,0:T(8,128)(2,1)S(1)}, u32[]{:S(2)}, u32[]{:S(2)}) async-start(bf16[16,6,768]{2,1,0:T(8,128)(2,1)} %copy.60), calls=%async_computation.4 | async-start | bytes 393216 | tf_op jit(solution)/shard_map/all_to_all | solution.py:134
Sparse Core Ops, SparseCore 0:
  74.3 16.7 reduce-scatter.6
  170.6 11.0 reduce-scatter.4
where the time goes:
time: 207 us; the launch traced here: 206 us
  blocking collectives  69 us (33%)
  waiting for transfers between devices  49.8 us (24%)
  local copies, waits for them, and re-layouts  32.9 us (16%)
  matrix products  16.7 us (8%)
  between operations  14.4 us (7%)
  starting transfers between devices  12.8 us (6%)
  other arithmetic  10.9 us (5%)
    unnamed x27, local copies, waits for them, and re-layouts  27.2 us
    all_gather x1, blocking collectives, shards(): rows_piece = lax.all_gather(own_rows, 'ep', axis=0, tiled=True)  24.1 us
    all_gather x1, blocking collectives, shards(): lax.all_gather(heads_out, 'ep', axis=0, tiled=True)  22.4 us
    unnamed x3, waiting for transfers between devices  16.6 us
    all_to_all x1, blocking collectives, shards(): lax.all_to_all(buffer, 'ep', split_axis=0, concat_axis=0, tiled=True)  14.8 us
    all_to_all x1, waiting for transfers between devices, shards(): lax.all_to_all(partial_proj, 'ep', split_axis=0, concat_axis=2, tiled=True)  13.2 us
    reduce_scatter x1, waiting for transfers between devices, shards(): lax.psum_scatter(down_part.astype(jnp.bfloat16), 'tp', scatter_dimension=...  11 us
    dot_general x1, matrix products, recurrence(): jnp.einsum('shk,shkv->shv', query_act, state_next, precision=lax.Precisio...  8.93 us
  transfers between devices with their start and end apart: 5, of which 5 were waited for; matrix products, arithmetic and copies ran while one was open for 4% of the time, Pallas kernels for 0%

commit v1 on v0

v1 whole, which is shorter than its diff:
```python
import functools

import jax
import jax.numpy as jnp
from jax import lax
from jax.experimental import pallas as pl
from jax.experimental.pallas import tpu as pltpu
from jax.sharding import PartitionSpec as P

rms_eps = 1e-06
MESH = pl.DeviceIdType.MESH
BF16 = jnp.bfloat16
F32 = jnp.float32
LANES = 128
ROWS = 16
SLOTS = 8


def rms_scale(values, gain):
    return values * lax.rsqrt(jnp.mean(values * values, axis=-1, keepdims=True) + rms_eps) * gain


def silu(values):
    return values * jax.nn.sigmoid(values)


def layer_kernel(
    n,
    tpn,
    residual_ref,
    mix_gain_ref,
    lower_ref,
    head_gain_ref,
    ffn_gain_ref,
    ids_ref,
    weight_ref,
    state_hbm,
    wq_hbm,
    wf_hbm,
    wi_hbm,
    wg_hbm,
    wo_hbm,
    eg_hbm,
    eu_hbm,
    ed_hbm,
    out_ref,
    new_hbm,
    wproj,
    wout,
    state,
    egate,
    eup,
    edown,
    resid,
    full,
    gath1,
    part2,
    recv2,
    perm,
    forget_s,
    query_s,
    value_s,
    gate_s,
    read_s,
    heads_s,
    gath3,
    part4,
    recv4,
    ids16,
    wts16,
    send5,
    recv5,
    part6,
    recv6,
    mix_s,
    load_sem,
    send_sem,
    recv_sem,
):
    me = lax.axis_index("ep")
    tp = lax.axis_index("tp")
    seq, width = residual_ref.shape
    quarter = width // tpn
    block = width // n
    nb = n // tpn
    heads = state.shape[1]

    barrier = pltpu.get_barrier_semaphore()

    def greet(i, carry):
        for j in range(tpn):
            other = lax.rem(me + i, n)
            pl.semaphore_signal(
                barrier, inc=1, device_id=(other, lax.rem(tp + j, tpn)), device_id_type=MESH
            )
        return carry

    for j in range(1, tpn):
        pl.semaphore_signal(
            barrier, inc=1, device_id=(me, lax.rem(tp + j, tpn)), device_id_type=MESH
        )
    lax.fori_loop(1, n, greet, 0)

    loads = [
        pltpu.make_async_copy(src, dst, load_sem.at[i])
        for i, (src, dst) in enumerate(
            [
                (wq_hbm, wproj.at[0]),
                (wf_hbm, wproj.at[1]),
                (wi_hbm, wproj.at[2]),
                (wg_hbm, wproj.at[3]),
                (state_hbm, state),
                (wo_hbm, wout),
                (eg_hbm, egate),
                (eu_hbm, eup),
                (ed_hbm, edown),
            ]
        )
    ]
    for load in loads:
        load.start()

    def remote(src, dst, phase, ep_to, tp_to):
        return pltpu.make_async_remote_copy(
            src_ref=src,
            dst_ref=dst,
            send_sem=send_sem.at[phase],
            recv_sem=recv_sem.at[phase],
            device_id=(ep_to, tp_to),
            device_id_type=MESH,
        )

    def drain(ref, sem):
        pltpu.make_async_copy(ref, ref, sem).wait()

    resid[...] = jnp.zeros_like(resid)
    resid[0:seq, :] = residual_ref[...].astype(F32)
    full[...] = rms_scale(resid[...], mix_gain_ref[...])
    own = pl.ds(pl.multiple_of(tp * quarter, LANES), quarter)
    gath1[me] = full[:, own].astype(BF16)

    pl.semaphore_wait(barrier, n * tpn - 1)

    def gather_start(buf, phase):
        def body(i, carry):
            remote(buf.at[me], buf.at[me], phase, lax.rem(me + i, n), tp).start()
            return carry

        lax.fori_loop(1, n, body, 0)

    gather_start(gath1, 0)

    part2[...] = jnp.zeros_like(part2)
    part4[...] = jnp.zeros_like(part4)
    read_s[...] = jnp.zeros_like(read_s)

    def perm_block(b, carry):
        lane = lax.broadcasted_iota(jnp.int32, (LANES, quarter), 0)
        col = lax.broadcasted_iota(jnp.int32, (LANES, quarter), 1)
        hit = jnp.logical_and(lane < block, col == lane + b * block)
        perm[pl.ds(pl.multiple_of(b * LANES, LANES), LANES), :] = jnp.where(hit, 1.0, 0.0).astype(
            BF16
        )
        return carry

    lax.fori_loop(0, nb, perm_block, 0)

    ids16[...] = jnp.full(ids16.shape, -1, jnp.int32)
    ids16[0:seq, :] = ids_ref[...]
    wts16[...] = jnp.zeros_like(wts16)
    wts16[0:seq, :] = weight_ref[...]
    lane8 = lax.broadcasted_iota(jnp.int32, (ROWS, n * SLOTS), 1)
    expert_of = lane8 // SLOTS
    slot_of = lane8 % SLOTS
    member = jnp.zeros((ROWS, n * SLOTS), F32)
    weighted = jnp.zeros((ROWS, n * SLOTS), F32)
    for k in range(ids_ref.shape[1]):
        same = ids16[:, k : k + 1] == expert_of
        member = member + jnp.where(same, 1.0, 0.0)
        weighted = weighted + jnp.where(same, wts16[:, k : k + 1], 0.0)
    row_i = lax.broadcasted_iota(jnp.int32, (ROWS, ROWS), 0)
    row_j = lax.broadcasted_iota(jnp.int32, (ROWS, ROWS), 1)
    earlier = jnp.where(row_j < row_i, 1.0, 0.0).astype(BF16)
    rank = jnp.dot(earlier, member.astype(BF16), preferred_element_type=F32)
    in_slot = jnp.where(rank == slot_of.astype(F32), 1.0, 0.0)
    placer = (member * in_slot).T.astype(BF16)
    weighted = weighted * in_slot
    weight_hi = weighted.astype(BF16)
    weight_lo = (weighted - weight_hi.astype(F32)).astype(BF16)

    for load in loads[:4]:
        load.wait()
    drain(gath1.at[pl.ds(0, n - 1)], recv_sem.at[0])
    rows1 = gath1[...].reshape(n * ROWS, quarter)
    for j in range(4):
        product = jnp.dot(rows1, wproj[j], preferred_element_type=F32)
        part2[:, j, :, 0:block] = product.reshape(n, ROWS, block).astype(BF16)
    target = me // nb
    place = lax.rem(me, nb)

    @pl.when(target == tp)
    def _():
        pltpu.make_async_copy(part2.at[me], recv2.at[tp, place], recv_sem.at[1]).start()

    @pl.when(target != tp)
    def _():
        remote(part2.at[me], recv2.at[tp, place], 1, me, target).start()

    def send2(i, carry):
        to = lax.rem(me + i, n)
        remote(part2.at[to], recv2.at[tp, place], 1, to, target).start()
        return carry

    lax.fori_loop(1, n, send2, 0)
    loads[4].wait()
    drain(recv2, recv_sem.at[1])
    projected = jnp.zeros((4 * ROWS, quarter), F32)
    for t in range(tpn):
        lhs = jnp.concatenate(
            [recv2[t, b].reshape(4 * ROWS, LANES) for b in range(nb)], axis=1
        )
        projected = projected + jnp.dot(lhs, perm[...], preferred_element_type=F32)
    projected = projected.astype(BF16).astype(F32)
    query_s[...] = silu(projected[0:ROWS])
    lower = lower_ref[...]
    forget_s[...] = lower + (1.0 - lower) * jax.nn.sigmoid(projected[ROWS : 2 * ROWS])
    value_s[...] = projected[2 * ROWS : 3 * ROWS]
    gate_s[...] = silu(projected[3 * ROWS : 4 * ROWS])

    def one_head(h, carry):
        cols = pl.ds(pl.multiple_of(h * LANES, LANES), LANES)
        forget_t = forget_s[:, cols].T
        query_t = query_s[:, cols].T
        for s in range(seq):
            value = value_s[s : s + 1, cols]
            updated = value + forget_t[:, s : s + 1] * (state[s, h].astype(F32) - value)
            state[s, h] = updated.astype(BF16)
            read_s[s : s + 1, cols] = jnp.sum(query_t[:, s : s + 1] * updated, 0, keepdims=True)
        heads_s[:, cols] = rms_scale(read_s[:, cols], head_gain_ref[...]) * gate_s[:, cols]
        return carry

    lax.fori_loop(0, heads, one_head, 0)
    gath3[me] = heads_s[...].astype(BF16)
    gather_start(gath3, 2)
    store = pltpu.make_async_copy(state, new_hbm, load_sem.at[9])
    store.start()

    loads[5].wait()
    drain(gath3.at[pl.ds(0, n - 1)], recv_sem.at[2])
    rows3 = gath3[...].reshape(n * ROWS, quarter)
    product = jnp.dot(rows3, wout[...], preferred_element_type=F32)
    part4[:, :, 0:block] = product.reshape(n, ROWS, block).astype(BF16)
    mine = tp * n + me
    recv4[mine] = part4[me]
    for j in range(1, tpn):
        remote(part4.at[me], recv4.at[mine], 3, me, lax.rem(tp + j, tpn)).start()

    def send4(i, carry):
        to = lax.rem(me + i, n)
        for j in range(tpn):
            remote(part4.at[to], recv4.at[mine], 3, to, lax.rem(tp + j, tpn)).start()
        return carry

    lax.fori_loop(1, n, send4, 0)
    drain(recv4.at[pl.ds(0, n * tpn - 1)], recv_sem.at[3])
    for half in range(tpn):
        mixed = jnp.zeros((ROWS, quarter), F32)
        for t in range(tpn):
            lhs = jnp.concatenate([recv4[t * n + half * nb + b] for b in range(nb)], axis=1)
            mixed = mixed + jnp.dot(lhs, perm[...], preferred_element_type=F32)
        cols = slice(half * quarter, (half + 1) * quarter)
        mix_s[:, cols] = (resid[:, cols] + mixed).astype(BF16).astype(F32)
    normed_ffn = rms_scale(mix_s[...], ffn_gain_ref[...]).astype(BF16)

    routed = jnp.dot(placer, normed_ffn, preferred_element_type=F32)
    send5[...] = routed.reshape(n, SLOTS, width).astype(BF16)
    recv5[me] = send5[me]

    def send_rows(i, carry):
        to = lax.rem(me + i, n)
        remote(send5.at[to], recv5.at[me], 4, to, tp).start()
        return carry

    lax.fori_loop(1, n, send_rows, 0)
    for load in loads[6:]:
        load.wait()
    drain(recv5.at[pl.ds(0, n - 1)], recv_sem.at[4])
    rows5 = recv5[...].astype(F32).reshape(n * SLOTS, width).astype(BF16)
    gate_part = jnp.dot(rows5, egate[0], preferred_element_type=F32)
    up_part = jnp.dot(rows5, eup[0], preferred_element_type=F32)
    hidden = (silu(gate_part) * up_part).astype(BF16)
    for t in range(tpn):
        down = jnp.dot(
            hidden, edown[0, :, t * quarter : (t + 1) * quarter], preferred_element_type=F32
        )
        part6[t] = down.reshape(n, SLOTS, quarter).astype(BF16)
    recv6[mine] = part6[tp, me]
    for j in range(1, tpn):
        to_tp = lax.rem(tp + j, tpn)
        remote(part6.at[to_tp, me], recv6.at[mine], 5, me, to_tp).start()

    def send6(i, carry):
        to = lax.rem(me + i, n)
        for j in range(tpn):
            to_tp = lax.rem(tp + j, tpn)
            remote(part6.at[to_tp, to], recv6.at[mine], 5, to, to_tp).start()
        return carry

    lax.fori_loop(1, n, send6, 0)
    drain(recv6.at[pl.ds(0, n * tpn - 1)], recv_sem.at[5])
    total = mix_s[:, own]
    for t in range(tpn):
        back = (
            recv6[t * n : (t + 1) * n].astype(F32).reshape(n * SLOTS, quarter).astype(BF16)
        )
        total = total + jnp.dot(weight_hi, back, preferred_element_type=F32)
        total = total + jnp.dot(weight_lo, back, preferred_element_type=F32)
    out_ref[...] = total[0:seq].astype(BF16)

    drain(gath1.at[pl.ds(0, n - 1)], send_sem.at[0])
    drain(part2.at[pl.ds(0, n - 1)], send_sem.at[1])

    @pl.when(target != tp)
    def _():
        drain(part2.at[0], send_sem.at[1])

    drain(gath3.at[pl.ds(0, n - 1)], send_sem.at[2])
    drain(recv4.at[pl.ds(0, n * tpn - 1)], send_sem.at[3])
    drain(send5.at[pl.ds(0, n - 1)], send_sem.at[4])
    drain(recv6.at[pl.ds(0, n * tpn - 1)], send_sem.at[5])
    store.wait()


def shards(
    residual_in,
    rec_state,
    mix_gain,
    w_query,
    w_forget,
    w_input,
    w_gate,
    lower_bound,
    head_gain,
    w_out,
    ffn_gain,
    route_ids,
    route_weight,
    expert_gate,
    expert_up,
    expert_down,
):
    tpn = lax.axis_size("tp")
    n = lax.axis_size("ep")
    seq, width = residual_in.shape
    quarter = width // tpn
    nb = n // tpn
    top = route_ids.shape[1]
    vmem = pl.BlockSpec(memory_space=pltpu.VMEM)
    hbm = pl.BlockSpec(memory_space=pl.ANY)
    rows_f32 = pltpu.VMEM((ROWS, quarter), F32)
    scratch = [
        pltpu.VMEM((4,) + w_query.shape, BF16),
        pltpu.VMEM(w_out.shape, BF16),
        pltpu.VMEM(rec_state.shape, BF16),
        pltpu.VMEM(expert_gate.shape, BF16),
        pltpu.VMEM(expert_up.shape, BF16),
        pltpu.VMEM(expert_down.shape, BF16),
        pltpu.VMEM((ROWS, width), F32),
        pltpu.VMEM((ROWS, width), F32),
        pltpu.VMEM((n, ROWS, quarter), BF16),
        pltpu.VMEM((n, 4, ROWS, LANES), BF16),
        pltpu.VMEM((tpn, nb, 4, ROWS, LANES), BF16),
        pltpu.VMEM((nb * LANES, quarter), BF16),
        rows_f32,
        rows_f32,
        rows_f32,
        rows_f32,
        rows_f32,
        rows_f32,
        pltpu.VMEM((n, ROWS, quarter), BF16),
        pltpu.VMEM((n, ROWS, LANES), BF16),
        pltpu.VMEM((tpn * n, ROWS, LANES), BF16),
        pltpu.VMEM((ROWS, top), jnp.int32),
        pltpu.VMEM((ROWS, top), F32),
        pltpu.VMEM((n, SLOTS, width), BF16),
        pltpu.VMEM((n, SLOTS, width), BF16),
        pltpu.VMEM((tpn, n, SLOTS, quarter), BF16),
        pltpu.VMEM((tpn * n, SLOTS, quarter), BF16),
        pltpu.VMEM((ROWS, width), F32),
        pltpu.SemaphoreType.DMA((10,)),
        pltpu.SemaphoreType.DMA((6,)),
        pltpu.SemaphoreType.DMA((6,)),
    ]
    return pl.pallas_call(
        functools.partial(layer_kernel, n, tpn),
        out_shape=(
            jax.ShapeDtypeStruct((seq, quarter), BF16),
            jax.ShapeDtypeStruct(rec_state.shape, BF16),
        ),
        in_specs=[vmem] * 7 + [hbm] * 9,
        out_specs=(vmem, hbm),
        scratch_shapes=scratch,
        compiler_params=pltpu.CompilerParams(
            collective_id=0, has_side_effects=True, vmem_limit_bytes=60 * 1024 * 1024
        ),
    )(
        residual_in,
        mix_gain.reshape(1, -1),
        lower_bound.reshape(1, -1),
        head_gain.reshape(1, -1),
        ffn_gain.reshape(1, -1),
        route_ids,
        route_weight,
        rec_state,
        w_query,
        w_forget,
        w_input,
        w_gate,
        w_out,
        expert_gate,
        expert_up,
        expert_down,
    )


def solution(mesh):
    in_specs = (
        P("ep", None),
        P("ep", "tp", None, None),
        P(),
        P("tp", "ep"),
        P("tp", "ep"),
        P("tp", "ep"),
        P("tp", "ep"),
        P("tp"),
        P(),
        P("tp", "ep"),
        P(),
        P("ep", None),
        P("ep", None),
        P("ep", None, "tp"),
        P("ep", None, "tp"),
        P("ep", "tp", None),
    )
    out_specs = (P("ep", "tp"), P("ep", "tp", None, None))
    return jax.shard_map(shards, mesh=mesh, in_specs=in_specs, out_specs=out_specs, check_vma=False)
```

time: 207 us -> 90 us (0.43)
  the two profiles are of different devices: /device:TPU:0 before, /device:TPU:29 now
where the time goes in v1:
time: 90 us; the launch traced here: 89.4 us
  Pallas kernels  68.3 us (76%)
  local copies, waits for them, and re-layouts  20.4 us (23%)
    pallas_call x1, Pallas kernels, shards(): pl.pallas_call(functools.partial(layer_kernel, n, tpn), out_shape=(jax.Sh...  68.3 us
    unnamed x9, local copies, waits for them, and re-layouts  16.6 us

profile of v1, /device:TPU:29, one launch (start us, length us, event | category | flops | bytes accessed | tf_op | source)
XLA Modules:
  0.0 89.4 jit_solution(7028450854700510047)
XLA Ops:
  0.6 1.3 %reshape.17.lower_ref = f32[1,768]{1,0:T(1,128)} reshape(f32[768]{0:T(1024)} %param.23) | data formatting | bytes 6144 | tf_op jit(solution)/shard_map/reshape | solution.py:409
  1.9 1.3 %reshape.16.mix_gain_ref = f32[1,1536]{1,0:T(1,128)} reshape(f32[1536]{0:T(1024)} %param.18) | data formatting | bytes 12288 | tf_op jit(solution)/shard_map/reshape | solution.py:408
  3.2 1.3 %reshape.19.ffn_gain_ref = f32[1,1536]{1,0:T(1,128)} reshape(f32[1536]{0:T(1024)} %param.26) | data formatting | bytes 12288 | tf_op jit(solution)/shard_map/reshape | solution.py:411
  4.5 1.4 %copy.18.ids_ref = s32[15,6]{1,0:T(8,128)} copy(s32[15,6]{0,1:T(8,128)} %param.27) | data formatting | bytes 720 | tf_op args[11]
  5.9 1.4 %copy.19.weight_ref = f32[15,6]{1,0:T(8,128)} copy(f32[15,6]{0,1:T(8,128)} %param.28) | data formatting | bytes 720 | tf_op args[12]
  7.2 1.7 %copy.20.wq_hbm = bf16[768,96]{1,0:T(8,128)(2,1)} copy(bf16[768,96]{0,1:T(8,128)(2,1)} %param.19) | data formatting | bytes 294912 | tf_op args[3]
  8.9 1.8 %copy.21.wf_hbm = bf16[768,96]{1,0:T(8,128)(2,1)} copy(bf16[768,96]{0,1:T(8,128)(2,1)} %param.20) | data formatting | bytes 294912 | tf_op args[4]
  10.7 1.7 %copy.22.wi_hbm = bf16[768,96]{1,0:T(8,128)(2,1)} copy(bf16[768,96]{0,1:T(8,128)(2,1)} %param.21) | data formatting | bytes 294912 | tf_op args[5]
  12.4 1.7 %copy.23.wg_hbm = bf16[768,96]{1,0:T(8,128)(2,1)} copy(bf16[768,96]{0,1:T(8,128)(2,1)} %param.22) | data formatting | bytes 294912 | tf_op args[6]
  14.2 1.7 %copy.24.wo_hbm = bf16[768,96]{1,0:T(8,128)(2,1)} copy(bf16[768,96]{0,1:T(8,128)(2,1)} %param.25) | data formatting | bytes 294912 | tf_op args[9]
  15.9 68.3 %shard_map.167 = (bf16[15,768]{1,0:T(8,128)(2,1)}, bf16[15,6,128,128]{3,2,1,0:T(8,128)(2,1)}) custom-call(bf16[15,1536]{1,0:T(8,128)(2,1)} %residual_ref.1, f32[1,1536]{1,0:T(1,128)} %reshape.16.mix_gain_ref, f32[1,768]{1,0:T(1,128)} %reshape.17.lower_ref, f32[1,128]{1,0:T(1,128)} %bitcast.1, f32[1,1536]{1,0:T(1,128)} %reshape.19.ffn_gain_ref, ...), custom_call_target="tpu_custom_call" | custom-call | tf_op jit(solution)/shard_map/pallas_call | solution.py:394
  84.2 1.3 %copy.27 = bf16[15,768]{1,0:T(8,128)(2,1)} copy(bf16[15,768]{1,0:T(8,128)(2,1)} %get-tuple-element.4) | data formatting | bytes 46080
  85.6 3.8 %copy.28 = bf16[15,6,128,128]{3,2,1,0:T(8,128)(2,1)} copy(bf16[15,6,128,128]{3,2,1,0:T(8,128)(2,1)} %get-tuple-element.5) | data formatting | bytes 5898240

commit v2 on v1

--- a/solution.py
+++ b/solution.py
@@ -44,8 +44,9 @@
     eu_hbm,
     ed_hbm,
     out_ref,
-    new_hbm,
+    new_ref,
     wproj,
+    wraw,
     wout,
     state,
     egate,
@@ -84,6 +85,11 @@
     block = width // n
     nb = n // tpn
     heads = state.shape[1]
+    chips = n // 2
+    wide = wproj.shape[0]
+    chip = me // 2
+    core = lax.rem(me, 2)
+    sibling = chip * 2 + 1 - core
 
     barrier = pltpu.get_barrier_semaphore()
 
@@ -101,14 +107,21 @@
         )
     lax.fori_loop(1, n, greet, 0)
 
+    step = -(-block // 16) * 16
+    if step == block:
+        landing = [wproj.at[pl.ds(j * block, block)] for j in range(4)]
+    else:
+        landing = [wraw.at[j] for j in range(4)]
+    if wide > 4 * block:
+        wproj[...] = jnp.zeros_like(wproj)
     loads = [
         pltpu.make_async_copy(src, dst, load_sem.at[i])
         for i, (src, dst) in enumerate(
             [
-                (wq_hbm, wproj.at[0]),
-                (wf_hbm, wproj.at[1]),
-                (wi_hbm, wproj.at[2]),
-                (wg_hbm, wproj.at[3]),
+                (wq_hbm, landing[0]),
+                (wf_hbm, landing[1]),
+                (wi_hbm, landing[2]),
+                (wg_hbm, landing[3]),
                 (state_hbm, state),
                 (wo_hbm, wout),
                 (eg_hbm, egate),
@@ -135,22 +148,29 @@
 
     resid[...] = jnp.zeros_like(resid)
     resid[0:seq, :] = residual_ref[...].astype(F32)
-    full[...] = rms_scale(resid[...], mix_gain_ref[...])
+    full[...] = rms_scale(resid[...], mix_gain_ref[...][None, :])
     own = pl.ds(pl.multiple_of(tp * quarter, LANES), quarter)
-    gath1[me] = full[:, own].astype(BF16)
+    gath1[core, chip] = full[:, own].astype(BF16)
 
     pl.semaphore_wait(barrier, n * tpn - 1)
 
     def gather_start(buf, phase):
         def body(i, carry):
-            remote(buf.at[me], buf.at[me], phase, lax.rem(me + i, n), tp).start()
+            to = lax.rem(chip + i, chips) * 2 + core
+            remote(buf.at[core, chip], buf.at[core, chip], phase, to, tp).start()
             return carry
 
-        lax.fori_loop(1, n, body, 0)
+        lax.fori_loop(1, chips, body, 0)
+
+    def gather_finish(buf, phase, half_done):
+        drain(buf.at[core, pl.ds(0, chips - 1)], recv_sem.at[phase])
+        remote(buf.at[core], buf.at[core], phase + 1, sibling, tp).start()
+        half_done(core)
+        drain(buf.at[core], recv_sem.at[phase + 1])
+        half_done(1 - core)
 
     gather_start(gath1, 0)
 
-    part2[...] = jnp.zeros_like(part2)
     part4[...] = jnp.zeros_like(part4)
     read_s[...] = jnp.zeros_like(read_s)
 
@@ -166,63 +186,82 @@
     lax.fori_loop(0, nb, perm_block, 0)
 
     ids16[...] = jnp.full(ids16.shape, -1, jnp.int32)
-    ids16[0:seq, :] = ids_ref[...]
+    ids16[:, 0:seq] = ids_ref[...]
     wts16[...] = jnp.zeros_like(wts16)
-    wts16[0:seq, :] = weight_ref[...]
-    lane8 = lax.broadcasted_iota(jnp.int32, (ROWS, n * SLOTS), 1)
-    expert_of = lane8 // SLOTS
-    slot_of = lane8 % SLOTS
-    member = jnp.zeros((ROWS, n * SLOTS), F32)
-    weighted = jnp.zeros((ROWS, n * SLOTS), F32)
-    for k in range(ids_ref.shape[1]):
-        same = ids16[:, k : k + 1] == expert_of
+    wts16[:, 0:seq] = weight_ref[...]
+    row8 = lax.broadcasted_iota(jnp.int32, (n * SLOTS, ROWS), 0)
+    expert_of = row8 // SLOTS
+    slot_of = row8 % SLOTS
+    member = jnp.zeros((n * SLOTS, ROWS), F32)
+    weighted = jnp.zeros((n * SLOTS, ROWS), F32)
+    for k in range(ids_ref.shape[0]):
+        same = ids16[k : k + 1, :] == expert_of
         member = member + jnp.where(same, 1.0, 0.0)
-        weighted = weighted + jnp.where(same, wts16[:, k : k + 1], 0.0)
+        weighted = weighted + jnp.where(same, wts16[k : k + 1, :], 0.0)
     row_i = lax.broadcasted_iota(jnp.int32, (ROWS, ROWS), 0)
     row_j = lax.broadcasted_iota(jnp.int32, (ROWS, ROWS), 1)
-    earlier = jnp.where(row_j < row_i, 1.0, 0.0).astype(BF16)
-    rank = jnp.dot(earlier, member.astype(BF16), preferred_element_type=F32)
+    earlier = jnp.where(row_i < row_j, 1.0, 0.0).astype(BF16)
+    rank = jnp.dot(member.astype(BF16), earlier, preferred_element_type=F32)
     in_slot = jnp.where(rank == slot_of.astype(F32), 1.0, 0.0)
-    placer = (member * in_slot).T.astype(BF16)
-    weighted = weighted * in_slot
+    placer = (member * in_slot).astype(BF16)
+    weighted = (weighted * in_slot).T
     weight_hi = weighted.astype(BF16)
     weight_lo = (weighted - weight_hi.astype(F32)).astype(BF16)
 
     for load in loads[:4]:
         load.wait()
-    drain(gath1.at[pl.ds(0, n - 1)], recv_sem.at[0])
-    rows1 = gath1[...].reshape(n * ROWS, quarter)
-    for j in range(4):
-        product = jnp.dot(rows1, wproj[j], preferred_element_type=F32)
-        part2[:, j, :, 0:block] = product.reshape(n, ROWS, block).astype(BF16)
+    if step != block:
+        for j in range(4):
+            wproj[j * step : j * step + block, :] = wraw[j]
     target = me // nb
     place = lax.rem(me, nb)
 
+    def project(side):
+        rows = gath1[side].reshape(chips * ROWS, quarter)
+        product = lax.dot_general(
+            rows, wproj[...], (((1,), (1,)), ((), ())), preferred_element_type=F32
+        )
+        part2[side] = product.reshape(chips, ROWS, wide).astype(BF16)
+
+    gather_finish(gath1, 0, project)
+
     @pl.when(target == tp)
     def _():
-        pltpu.make_async_copy(part2.at[me], recv2.at[tp, place], recv_sem.at[1]).start()
+        pltpu.make_async_copy(part2.at[core, chip], recv2.at[tp, place], recv_sem.at[6]).start()
 
     @pl.when(target != tp)
     def _():
-        remote(part2.at[me], recv2.at[tp, place], 1, me, target).start()
+        remote(part2.at[core, chip], recv2.at[tp, place], 6, me, target).start()
 
     def send2(i, carry):
         to = lax.rem(me + i, n)
-        remote(part2.at[to], recv2.at[tp, place], 1, to, target).start()
+        remote(part2.at[lax.rem(to, 2), to // 2], recv2.at[tp, place], 6, to, target).start()
         return carry
 
     lax.fori_loop(1, n, send2, 0)
     loads[4].wait()
-    drain(recv2, recv_sem.at[1])
-    projected = jnp.zeros((4 * ROWS, quarter), F32)
-    for t in range(tpn):
-        lhs = jnp.concatenate(
-            [recv2[t, b].reshape(4 * ROWS, LANES) for b in range(nb)], axis=1
-        )
-        projected = projected + jnp.dot(lhs, perm[...], preferred_element_type=F32)
+    drain(recv2, recv_sem.at[6])
+    blocks = recv2[...].astype(F32).reshape(n * ROWS, wide)
+    shifted = []
+    for j in range(4):
+        moved = pltpu.roll(blocks, (wide - j * step) % wide, 1) if j else blocks
+        shifted.append(moved[:, 0:LANES].astype(BF16).reshape(tpn, nb, ROWS, LANES))
+    lhs = jnp.concatenate(
+        [
+            jnp.concatenate([shifted[j][t, b] for b in range(nb)], axis=1)
+            for t in range(tpn)
+            for j in range(4)
+        ],
+        axis=0,
+    )
+    placed = jnp.dot(lhs, perm[...], preferred_element_type=F32)
+    placed = placed.reshape(tpn, 4 * ROWS, quarter)
+    projected = placed[0]
+    for t in range(1, tpn):
+        projected = projected + placed[t]
     projected = projected.astype(BF16).astype(F32)
     query_s[...] = silu(projected[0:ROWS])
-    lower = lower_ref[...]
+    lower = lower_ref[...][None, :]
     forget_s[...] = lower + (1.0 - lower) * jax.nn.sigmoid(projected[ROWS : 2 * ROWS])
     value_s[...] = projected[2 * ROWS : 3 * ROWS]
     gate_s[...] = silu(projected[3 * ROWS : 4 * ROWS])
@@ -234,43 +273,57 @@
         for s in range(seq):
             value = value_s[s : s + 1, cols]
             updated = value + forget_t[:, s : s + 1] * (state[s, h].astype(F32) - value)
-            state[s, h] = updated.astype(BF16)
+            new_ref[s, h] = updated.astype(BF16)
             read_s[s : s + 1, cols] = jnp.sum(query_t[:, s : s + 1] * updated, 0, keepdims=True)
-        heads_s[:, cols] = rms_scale(read_s[:, cols], head_gain_ref[...]) * gate_s[:, cols]
+        heads_s[:, cols] = rms_scale(read_s[:, cols], head_gain_ref[...][None, :]) * gate_s[:, cols]
         return carry
 
     lax.fori_loop(0, heads, one_head, 0)
-    gath3[me] = heads_s[...].astype(BF16)
+    gath3[core, chip] = heads_s[...].astype(BF16)
     gather_start(gath3, 2)
-    store = pltpu.make_async_copy(state, new_hbm, load_sem.at[9])
-    store.start()
 
     loads[5].wait()
-    drain(gath3.at[pl.ds(0, n - 1)], recv_sem.at[2])
-    rows3 = gath3[...].reshape(n * ROWS, quarter)
-    product = jnp.dot(rows3, wout[...], preferred_element_type=F32)
-    part4[:, :, 0:block] = product.reshape(n, ROWS, block).astype(BF16)
+
+    def mix(side):
+        rows = gath3[side].reshape(chips * ROWS, quarter)
+        product = lax.dot_general(
+            rows, wout[...], (((1,), (1,)), ((), ())), preferred_element_type=F32
+        )
+        part4[side, :, :, 0:block] = product.reshape(chips, ROWS, block).astype(BF16)
+
+    gather_finish(gath3, 2, mix)
     mine = tp * n + me
-    recv4[mine] = part4[me]
+    recv4[mine] = part4[core, chip]
     for j in range(1, tpn):
-        remote(part4.at[me], recv4.at[mine], 3, me, lax.rem(tp + j, tpn)).start()
+        remote(part4.at[core, chip], recv4.at[mine], 7, me, lax.rem(tp + j, tpn)).start()
 
     def send4(i, carry):
         to = lax.rem(me + i, n)
         for j in range(tpn):
-            remote(part4.at[to], recv4.at[mine], 3, to, lax.rem(tp + j, tpn)).start()
+            remote(
+                part4.at[lax.rem(to, 2), to // 2], recv4.at[mine], 7, to, lax.rem(tp + j, tpn)
+            ).start()
         return carry
 
     lax.fori_loop(1, n, send4, 0)
-    drain(recv4.at[pl.ds(0, n * tpn - 1)], recv_sem.at[3])
+    drain(recv4.at[pl.ds(0, n * tpn - 1)], recv_sem.at[7])
+    lhs = jnp.concatenate(
+        [
+            jnp.concatenate([recv4[t * n + half * nb + b] for b in range(nb)], axis=1)
+            for t in range(tpn)
+            for half in range(tpn)
+        ],
+        axis=0,
+    )
+    placed = jnp.dot(lhs, perm[...], preferred_element_type=F32)
+    placed = placed.reshape(tpn, tpn, ROWS, quarter)
     for half in range(tpn):
-        mixed = jnp.zeros((ROWS, quarter), F32)
-        for t in range(tpn):
-            lhs = jnp.concatenate([recv4[t * n + half * nb + b] for b in range(nb)], axis=1)
-            mixed = mixed + jnp.dot(lhs, perm[...], preferred_element_type=F32)
+        mixed = placed[0, half]
+        for t in range(1, tpn):
+            mixed = mixed + placed[t, half]
         cols = slice(half * quarter, (half + 1) * quarter)
         mix_s[:, cols] = (resid[:, cols] + mixed).astype(BF16).astype(F32)
-    normed_ffn = rms_scale(mix_s[...], ffn_gain_ref[...]).astype(BF16)
+    normed_ffn = rms_scale(mix_s[...], ffn_gain_ref[...][None, :]).astype(BF16)
 
     routed = jnp.dot(placer, normed_ffn, preferred_element_type=F32)
     send5[...] = routed.reshape(n, SLOTS, width).astype(BF16)
@@ -317,18 +370,21 @@
         total = total + jnp.dot(weight_lo, back, preferred_element_type=F32)
     out_ref[...] = total[0:seq].astype(BF16)
 
-    drain(gath1.at[pl.ds(0, n - 1)], send_sem.at[0])
-    drain(part2.at[pl.ds(0, n - 1)], send_sem.at[1])
+    for buf, phase in ((gath1, 0), (gath3, 2)):
+        drain(buf.at[0, pl.ds(0, chips - 1)], send_sem.at[phase])
+        drain(buf.at[0], send_sem.at[phase + 1])
+    drain(recv2.at[0], send_sem.at[6])
+    for t in range(1, tpn - 1):
+        drain(recv2.at[0], send_sem.at[6])
+    drain(recv2.at[0, pl.ds(0, nb - 1)], send_sem.at[6])
 
     @pl.when(target != tp)
     def _():
-        drain(part2.at[0], send_sem.at[1])
-
-    drain(gath3.at[pl.ds(0, n - 1)], send_sem.at[2])
-    drain(recv4.at[pl.ds(0, n * tpn - 1)], send_sem.at[3])
+        drain(recv2.at[0, 0], send_sem.at[6])
+
+    drain(recv4.at[pl.ds(0, n * tpn - 1)], send_sem.at[7])
     drain(send5.at[pl.ds(0, n - 1)], send_sem.at[4])
     drain(recv6.at[pl.ds(0, n * tpn - 1)], send_sem.at[5])
-    store.wait()
 
 
 def shards(
@@ -355,21 +411,25 @@
     quarter = width // tpn
     nb = n // tpn
     top = route_ids.shape[1]
+    wide = -(-4 * (-(-width // n // 16) * 16) // LANES) * LANES
+    outputs = rec_state.size * 2 + ROWS * quarter * 2
+    limit = 67043328 - outputs - 8192
     vmem = pl.BlockSpec(memory_space=pltpu.VMEM)
     hbm = pl.BlockSpec(memory_space=pl.ANY)
     rows_f32 = pltpu.VMEM((ROWS, quarter), F32)
     scratch = [
-        pltpu.VMEM((4,) + w_query.shape, BF16),
-        pltpu.VMEM(w_out.shape, BF16),
+        pltpu.VMEM((wide, quarter), BF16),
+        pltpu.VMEM((4, width // n, quarter), BF16),
+        pltpu.VMEM((width // n, quarter), BF16),
         pltpu.VMEM(rec_state.shape, BF16),
         pltpu.VMEM(expert_gate.shape, BF16),
         pltpu.VMEM(expert_up.shape, BF16),
         pltpu.VMEM(expert_down.shape, BF16),
         pltpu.VMEM((ROWS, width), F32),
         pltpu.VMEM((ROWS, width), F32),
-        pltpu.VMEM((n, ROWS, quarter), BF16),
-        pltpu.VMEM((n, 4, ROWS, LANES), BF16),
-        pltpu.VMEM((tpn, nb, 4, ROWS, LANES), BF16),
+        pltpu.VMEM((2, n // 2, ROWS, quarter), BF16),
+        pltpu.VMEM((2, n // 2, ROWS, wide), BF16),
+        pltpu.VMEM((tpn, nb, ROWS, wide), BF16),
         pltpu.VMEM((nb * LANES, quarter), BF16),
         rows_f32,
         rows_f32,
@@ -377,46 +437,46 @@
         rows_f32,
         rows_f32,
         rows_f32,
-        pltpu.VMEM((n, ROWS, quarter), BF16),
-        pltpu.VMEM((n, ROWS, LANES), BF16),
+        pltpu.VMEM((2, n // 2, ROWS, quarter), BF16),
+        pltpu.VMEM((2, n // 2, ROWS, LANES), BF16),
         pltpu.VMEM((tpn * n, ROWS, LANES), BF16),
-        pltpu.VMEM((ROWS, top), jnp.int32),
-        pltpu.VMEM((ROWS, top), F32),
+        pltpu.VMEM((top, ROWS), jnp.int32),
+        pltpu.VMEM((top, ROWS), F32),
         pltpu.VMEM((n, SLOTS, width), BF16),
         pltpu.VMEM((n, SLOTS, width), BF16),
         pltpu.VMEM((tpn, n, SLOTS, quarter), BF16),
         pltpu.VMEM((tpn * n, SLOTS, quarter), BF16),
         pltpu.VMEM((ROWS, width), F32),
         pltpu.SemaphoreType.DMA((10,)),
-        pltpu.SemaphoreType.DMA((6,)),
-        pltpu.SemaphoreType.DMA((6,)),
+        pltpu.SemaphoreType.DMA((8,)),
+        pltpu.SemaphoreType.DMA((8,)),
     ]
     return pl.pallas_call(
         functools.partial(layer_kernel, n, tpn),
         out_shape=(
-            jax.ShapeDtypeStruct((seq, quarter), BF16),
-            jax.ShapeDtypeStruct(rec_state.shape, BF16),
+            pltpu.VMEM((seq, quarter), BF16),
+            pltpu.VMEM(rec_state.shape, BF16),
         ),
         in_specs=[vmem] * 7 + [hbm] * 9,
-        out_specs=(vmem, hbm),
+        out_specs=(vmem, vmem),
         scratch_shapes=scratch,
         compiler_params=pltpu.CompilerParams(
-            collective_id=0, has_side_effects=True, vmem_limit_bytes=60 * 1024 * 1024
+            collective_id=0, has_side_effects=True, vmem_limit_bytes=limit
         ),
     )(
         residual_in,
-        mix_gain.reshape(1, -1),
-        lower_bound.reshape(1, -1),
-        head_gain.reshape(1, -1),
-        ffn_gain.reshape(1, -1),
-        route_ids,
-        route_weight,
+        mix_gain,
+        lower_bound,
+        head_gain,
+        ffn_gain,
+        route_ids.T,
+        route_weight.T,
         rec_state,
-        w_query,
-        w_forget,
-        w_input,
-        w_gate,
-        w_out,
+        w_query.T,
+        w_forget.T,
+        w_input.T,
+        w_gate.T,
+        w_out.T,
         expert_gate,
         expert_up,
         expert_down,

time: 90 us -> 62.8 us (0.70)
  local copies, waits for them, and re-layouts: 20.4 us -> 2.21 us
  Pallas kernels: 68.3 us -> 59.6 us
    unnamed x9 -> x2, local copies, waits for them, and re-layouts: 16.6 us -> 2.21 us
    pallas_call x1, Pallas kernels: 68.3 us -> 59.6 us  [shards(): pl.pallas_call(functools.partial(layer_kernel, n, tpn), out_shape=(pltpu....]
    reshape x3 -> x0, local copies, waits for them, and re-layouts: 3.87 us -> none  [the longest x1 1.29 us: shards(): mix_gain.reshape(1, -1)]
where the time goes in v2:
time: 62.8 us; the launch traced here: 62.4 us
  Pallas kernels  59.6 us (95%)
  local copies, waits for them, and re-layouts  2.21 us (4%)
  between operations  0.65 us (1%)
    pallas_call x1, Pallas kernels, shards(): pl.pallas_call(functools.partial(layer_kernel, n, tpn), out_shape=(pltpu....  59.6 us
    unnamed x2, local copies, waits for them, and re-layouts  2.21 us

profile of v2, /device:TPU:29, one launch (start us, length us, event | category | flops | bytes accessed | tf_op | source)
XLA Modules:
  0.0 62.4 jit_solution(9281489816865929975)
XLA Ops:
  0.6 59.6 %shard_map.167 = (bf16[15,768]{1,0:T(8,128)(2,1)S(1)}, bf16[15,6,128,128]{3,2,1,0:T(8,128)(2,1)S(1)}) custom-call(bf16[15,1536]{1,0:T(8,128)(2,1)} %residual_ref.1, f32[1536]{0:T(1024)} %mix_gain_ref.1, f32[768]{0:T(1024)} %lower_ref.1, f32[128]{0:T(128)} %head_gain_ref.1, f32[1536]{0:T(1024)} %ffn_gain_ref.1, s32[6,15]{1,0:T(8,128)} %bitcast.12, ...), custom_call_target="tpu_custom_call" | custom-call | tf_op jit(solution)/shard_map/pallas_call | solution.py:454
  60.2 0.6 copy.20
  60.8 1.6 %copy.21 = bf16[15,6,128,128]{3,2,1,0:T(8,128)(2,1)} copy(bf16[15,6,128,128]{3,2,1,0:T(8,128)(2,1)S(1)} %get-tuple-element.3) | data formatting | bytes 5898240
